TPU v7x, 32 devices: a whole 2x2x4 slice. The times are simulated.
32 devices in a mesh: sp: 16 (over z, y, x), tp: 2 (over core).
Axes of the slice: x: 2, y: 2, z: 4, core: 2. Of those that a mesh axis runs over, the one named last changes fastest.
Arguments:
- resid: bfloat16 [3072, 2048], P('sp'), may hold values from -6 to 6
- queries: bfloat16 [3072, 1024], P('sp', 'tp'), may hold values from -6.5 to 6.5
- keys: bfloat16 [3072, 1024], P('sp', 'tp'), may hold values from -6.5 to 6.5
- values: bfloat16 [3072, 1024], P('sp', 'tp'), may hold values from -6 to 6
- lambdas: float32 [8], P('tp'), may hold values from 0.3 to 0.8
- head_gain: float32 [128], replicated, may hold values from 0.1 to 1.9
- out_weight: bfloat16 [1024, 2048], P('tp'), may hold values from -0.1875 to 0.1875
- norm_gain: float32 [2048], replicated, may hold values from 0.1 to 1.9
- gate_weight: bfloat16 [2048, 5632], P('sp', 'tp'), may hold values from -0.125 to 0.125
- up_weight: bfloat16 [2048, 5632], P('sp', 'tp'), may hold values from -0.125 to 0.125
- down_weight: bfloat16 [5632, 2048], P('tp', 'sp'), may hold values from -0.078125 to 0.078125
Outputs:
- result: bfloat16 [3072, 2048], P('sp')
All inputs are finite; a program needn't handle non-finite values.
Results may differ from a plain program's by a relative error of at most 0.014.
Values may be sent and summed in bfloat16 or wider, within the bound.
A program may use at most 128 MiB of HBM per device.

v0:
```python
import jax
import jax.numpy as jnp
from jax import lax
from jax.sharding import PartitionSpec as P

QK = 64
VD = 128


def rms_rows(first, norm_gain):
    return (
        first * lax.rsqrt(jnp.mean(first * first, axis=-1, keepdims=True) + 1e-06) * norm_gain
    ).astype(jnp.bfloat16)


def local(
    resid,
    queries,
    keys,
    values,
    lambdas,
    head_gain,
    out_weight,
    norm_gain,
    gate_weight,
    up_weight,
    down_weight,
):
    tok_rows = queries.shape[0]
    local_heads = lambdas.shape[0]
    model_width = resid.shape[1]
    offset = lax.axis_index("sp") * tok_rows
    query_four = queries.reshape(tok_rows, local_heads, 2, QK)
    score_scale = QK ** (-0.5)
    query_pos = offset + lax.iota(jnp.int32, tok_rows)
    last_query = offset + tok_rows - 1

    def update(fold_state, key_part, value_part, key_pos):
        run_max, run_sum, run_acc = fold_state
        scores = (
            jnp.einsum("qhcd,khcd->chqk", query_four, key_part, preferred_element_type=jnp.float32)
            * score_scale
        )
        causal_mask = key_pos[None, :] <= query_pos[:, None]
        scores = jnp.where(causal_mask, scores, -1e30)
        new_max = jnp.maximum(run_max, jnp.max(scores, axis=-1))
        expo = jnp.where(causal_mask, jnp.exp(scores - new_max[..., None]), 0.0)
        factor = jnp.exp(run_max - new_max)
        new_sum = run_sum * factor + jnp.sum(expo, axis=-1)
        new_acc = run_acc * factor[..., None] + jnp.einsum(
            "chqk,khd->chqd",
            expo.astype(jnp.bfloat16),
            value_part,
            preferred_element_type=jnp.float32,
        )
        return (new_max, new_sum, new_acc)

    initial = (
        jnp.full((2, local_heads, tok_rows), -1e30, jnp.float32),
        jnp.zeros((2, local_heads, tok_rows), jnp.float32),
        jnp.zeros((2, local_heads, tok_rows, VD), jnp.float32),
    )
    key_rows = lax.all_gather(keys, "sp", axis=0, tiled=True)
    value_rows = lax.all_gather(values, "sp", axis=0, tiled=True)
    key_count = key_rows.shape[0]
    key_span = key_count
    while key_span > 1024 and key_span % 2 == 0:
        key_span = key_span // 2

    def one_span(span_index, inner_state):
        span_start = span_index * key_span
        key_part = lax.dynamic_slice_in_dim(key_rows, span_start, key_span, 0).reshape(
            key_span, local_heads, 2, QK
        )
        value_part = lax.dynamic_slice_in_dim(value_rows, span_start, key_span, 0).reshape(
            key_span, local_heads, VD
        )
        key_pos = span_start + lax.iota(jnp.int32, key_span)
        return update(inner_state, key_part, value_part, key_pos)

    def run_spans(inner_state):
        return lax.fori_loop(0, key_count // key_span, one_span, inner_state)

    def keep_state(inner_state):
        return inner_state

    final_max, final_sum, final_acc = lax.cond(
        jnp.int32(0) <= last_query, run_spans, keep_state, initial
    )
    ratio = final_acc / final_sum[..., None]
    mixed_heads = ratio[0] - lambdas[:, None, None] * ratio[1]
    head_out = (
        mixed_heads
        * lax.rsqrt(jnp.mean(mixed_heads * mixed_heads, axis=-1, keepdims=True) + 1e-05)
        * head_gain
    ).astype(jnp.bfloat16)
    out_three = out_weight.reshape(local_heads, VD, model_width)
    own_count = tok_rows // lax.axis_size("tp")
    branch = lax.psum_scatter(
        jnp.einsum("hqd,hde->qe", head_out, out_three, preferred_element_type=jnp.float32).astype(
            jnp.bfloat16
        ),
        "tp",
        scatter_dimension=0,
        tiled=True,
    ).astype(jnp.float32)
    resid_own = lax.dynamic_slice_in_dim(resid, lax.axis_index("tp") * own_count, own_count, 0)
    first = resid_own.astype(jnp.float32) + branch
    normed_all = lax.all_gather(rms_rows(first, norm_gain), "tp", axis=0, tiled=True)
    gate_act = jnp.dot(
        normed_all,
        lax.all_gather(gate_weight, "sp", axis=0, tiled=True),
        preferred_element_type=jnp.float32,
    )
    up_act = jnp.dot(
        normed_all,
        lax.all_gather(up_weight, "sp", axis=0, tiled=True),
        preferred_element_type=jnp.float32,
    )
    hidden = (jax.nn.silu(gate_act) * up_act).astype(jnp.bfloat16)
    terms = jnp.dot(
        hidden,
        lax.all_gather(down_weight, "sp", axis=1, tiled=True),
        preferred_element_type=jnp.float32,
    )
    mixer = lax.psum_scatter(
        terms.astype(jnp.bfloat16), "tp", scatter_dimension=0, tiled=True
    ).astype(jnp.float32)
    finished = (first + 0.5 * mixer).astype(jnp.bfloat16)
    return lax.all_gather(finished, "tp", axis=0, tiled=True)


def solution(mesh):
    return jax.shard_map(
        local,
        mesh=mesh,
        in_specs=(
            P("sp", None),
            P("sp", "tp"),
            P("sp", "tp"),
            P("sp", "tp"),
            P("tp"),
            P(),
            P("tp", None),
            P(),
            P("sp", "tp"),
            P("sp", "tp"),
            P("tp", "sp"),
        ),
        out_specs=P("sp", None),
        check_vma=False,
    )
```

profile of v0, /device:TPU:25, one launch (start us, length us, event | category | flops | bytes accessed | tf_op | source)
XLA Modules:
  0.0 740.6 jit_solution(319168003058939454)
XLA Ops:
  8.1 68.9 %all-gather.6.cloned.1.call-done = bf16[3072,512]{1,0:T(8,128)(2,1)} async-done(((bf16[192,512]{1,0:T(8,128)(2,1)}), bf16[3072,512]{1,0:T(8,128)(2,1)}) %all-gather.6.cloned.1.call-update) | async-done | bytes 3145744 | tf_op jit(solution)/shard_map/all_gather | solution.py:63
  77.0 69.2 %all-gather.8.cloned.1.call-done = bf16[3072,512]{1,0:T(8,128)(2,1)} async-done(((bf16[192,512]{1,0:T(8,128)(2,1)}), bf16[3072,512]{1,0:T(8,128)(2,1)}) %all-gather.8.cloned.1.call-update) | async-done | bytes 3145744 | tf_op jit(solution)/shard_map/all_gather | solution.py:64
  146.2 78.7 %conditional.1 = (f32[2,4,192]{2,1,0:T(4,128)}, f32[2,4,192,128]{3,2,0,1:T(8,128)}) conditional(s32[]{:T(128)} %convert_element_type.38, () %tuple.27, (bf16[192,512]{1,0:T(8,128)(2,1)}, s32[]{:T(128)}, s32[192]{0:T(256)S(1)}, bf16[3072,512]{1,0:T(8,128)(2,1)}, bf16[3072,512]{1,0:T(8,128)(2,1)}) %tuple.28), branch_computations={%region_0.0_spmd, %region_1.6_spmd} | conditional | flops 464347584 | bytes 25131568 | solution.py:87
  147.3 77.6 %while.17 = (s32[]{:T(128)}, f32[2,4,192]{2,1,0:T(4,128)S(1)}, f32[2,4,192]{2,1,0:T(4,128)}, f32[2,4,192,128]{3,2,0,1:T(8,128)}, s32[192]{0:T(256)S(1)}, /*index...) while((s32[]{:T(128)}, f32[2,4,192]{2,1,0:T(4,128)S(1)}, ...), condition=%wide.region_5.5_spmd.clone, body=%wide.region_2.4_spmd.clone.sunk | while | flops 464347392 | bytes 24343476 | solution.py:82
  152.1 4.2 fusion.41
  156.4 4.3 fusion.42
  162.5 3.6 fusion.44
  170.9 4.2 fusion.41
  175.1 4.3 fusion.42
  181.9 3.7 fusion.44
  190.5 4.2 fusion.41
  194.7 4.3 fusion.42
  201.6 3.7 fusion.44
  210.1 4.2 fusion.41
  214.3 4.3 fusion.42
  221.2 3.7 fusion.44
  230.7 7.8 %reduce-scatter.3.cloned.1.call-done = bf16[96,2048]{1,0:T(8,128)(2,1)} async-done(((bf16[192,2048]{1,0:T(8,128)(2,1)}), bf16[96,2048]{1,0:T(8,128)(2,1)}) %reduce-scatter.3.cloned.1.call-update) | async-done | bytes 393232 | tf_op jit(solution)/shard_map/reduce_scatter | solution.py:99
  240.9 2.5 all_gather.23
  243.4 137.7 %all-gather.10.cloned.1.call-done = bf16[2048,2816]{1,0:T(8,128)(2,1)} async-done(((bf16[128,2816]{1,0:T(8,128)(2,1)}), bf16[2048,2816]{1,0:T(8,128)(2,1)}) %all-gather.10.cloned.1.call-update) | async-done | bytes 11534352 | tf_op jit(solution)/shard_map/all_gather | solution.py:112
  381.2 8.3 %fusion.22 = f32[192,2816]{1,0:T(8,128)} fusion(bf16[192,2048]{1,0:T(8,128)(2,1)} %all_gather.23, bf16[2048,2816]{1,0:T(8,128)(2,1)} %all-gather.10.cloned.1.call-done), kind=kOutput, calls=%fused_computation.42 | convolution fusion | flops 2214592512 | bytes 14483456 | tf_op jit(solution)/shard_map/dot_general | solution.py:110
  389.5 133.9 %all-gather.12.cloned.1.call-done = bf16[2048,2816]{1,0:T(8,128)(2,1)} async-done(((bf16[128,2816]{1,0:T(8,128)(2,1)}), bf16[2048,2816]{1,0:T(8,128)(2,1)}) %all-gather.12.cloned.1.call-update) | async-done | bytes 11534352 | tf_op jit(solution)/shard_map/all_gather | solution.py:117
  523.4 182.8 %all-gather.14.cloned.1.call-done = bf16[2816,2048]{1,0:T(8,128)(2,1)} async-done(((bf16[2816,128]{1,0:T(8,128)(2,1)}), bf16[2816,2048]{1,0:T(8,128)(2,1)}) %all-gather.14.cloned.1.call-update) | async-done | bytes 11534352 | tf_op jit(solution)/shard_map/all_gather | solution.py:123
  706.2 14.0 %convolution_convert_fusion = bf16[192,2048]{1,0:T(8,128)(2,1)} fusion(bf16[2816,2048]{1,0:T(8,128)(2,1)} %all-gather.14.cloned.1.call-done, bf16[192,2048]{1,0:T(8,128)(2,1)} %all_gather.23, bf16[2048,2816]{1,0:T(8,128)(2,1)} %all-gather.12.cloned.1.call-done, f32[192,2816]{1,0:T(8,128)} %fusion.22), kind=kOutput, calls=%fused_computation.25 | convolution fusion | flops 4432822272 | bytes 26804224 | tf_op jit(solution)/shard_map/dot_general | solution.py:121
  720.2 9.0 %reduce-scatter.5.cloned.1.call-done = bf16[96,2048]{1,0:T(8,128)(2,1)} async-done(((bf16[192,2048]{1,0:T(8,128)(2,1)}), bf16[96,2048]{1,0:T(8,128)(2,1)}) %reduce-scatter.5.cloned.1.call-update) | async-done | bytes 393232 | tf_op jit(solution)/shard_map/reduce_scatter | solution.py:126
  (80 shorter events, 43.6 us)
Async XLA Ops:
  6.5 220.8 %copy-start = (bf16[512,2048]{1,0:T(8,128)(2,1)S(1)}, bf16[512,2048]{1,0:T(8,128)(2,1)}, u32[]{:S(2)}) copy-start(bf16[512,2048]{1,0:T(8,128)(2,1)} %param.21) | copy-start | bytes 6291460
  6.5 70.4 %all-gather.6.cloned.1.call-start = ((), (), s32[]{:S(2)}) async-start(), calls=%async_computation.2 | async-start | bytes 3342336 | tf_op jit(solution)/shard_map/all_gather | solution.py:63
  7.3 138.9 %all-gather.8.cloned.1.call-start = ((), (), s32[]{:S(2)}) async-start(), calls=%async_computation.3 | async-start | bytes 3342336 | tf_op jit(solution)/shard_map/all_gather | solution.py:64
  8.0 230.5 %reduce-scatter.3.cloned.1.call-start = ((), (), s32[]{:S(2)}) async-start(), calls=%async_computation.4 | async-start | bytes 1179648 | tf_op jit(solution)/shard_map/reduce_scatter | solution.py:99
  146.2 80.8 %copy-start.4 = (f32[4]{0:T(128)S(1)}, f32[4]{0:T(128)}, u32[]{:S(2)}) copy-start(f32[4]{0:T(128)} %param.19) | copy-start | bytes 52
  146.2 81.2 %copy-start.5 = (f32[128]{0:T(128)S(1)}, f32[128]{0:T(128)}, u32[]{:S(2)}) copy-start(f32[128]{0:T(128)} %param.20) | copy-start | bytes 1540
  227.3 11.2 %copy-start.2 = (bf16[192,2048]{1,0:T(8,128)(2,1)S(1)}, bf16[192,2048]{1,0:T(8,128)(2,1)}, u32[]{:S(2)}) copy-start(bf16[192,2048]{1,0:T(8,128)(2,1)} %param.15) | copy-start | bytes 2359300
  227.4 12.4 %copy-start.3 = (f32[2048]{0:T(1024)S(1)}, f32[2048]{0:T(1024)}, u32[]{:S(2)}) copy-start(f32[2048]{0:T(1024)} %param.22) | copy-start | bytes 24580
  228.9 152.3 %all-gather.10.cloned.1.call-start = ((), (), s32[]{:S(2)}) async-start(), calls=%async_computation.5 | async-start | bytes 12255232 | tf_op jit(solution)/shard_map/all_gather | solution.py:112
  229.5 293.9 %all-gather.12.cloned.1.call-start = ((), (), s32[]{:S(2)}) async-start(), calls=%async_computation.6 | async-start | bytes 12255232 | tf_op jit(solution)/shard_map/all_gather | solution.py:117
  230.1 476.1 %all-gather.14.cloned.1.call-start = ((), (), s32[]{:S(2)}) async-start(), calls=%async_computation.7 | async-start | bytes 12255232 | tf_op jit(solution)/shard_map/all_gather | solution.py:123
  230.7 498.6 %reduce-scatter.5.cloned.1.call-start = ((), (), s32[]{:S(2)}) async-start(), calls=%async_computation.8 | async-start | bytes 1179648 | tf_op jit(solution)/shard_map/reduce_scatter | solution.py:126
  389.5 339.8 %copy-start.1 = (bf16[96,2048]{1,0:T(8,128)(2,1)S(1)}, bf16[96,2048]{1,0:T(8,128)(2,1)}, u32[]{:S(2)}) copy-start(bf16[96,2048]{1,0:T(8,128)(2,1)} %reduce-scatter.3.cloned.1.call-done) | copy-start | bytes 1179652
Sparse Core Ops, SparseCore 0:
  10.1 66.8 all-gather.5
  79.7 66.3 all-gather.7
  229.0 9.4 reduce-scatter.2
  241.1 139.9 all-gather.9
  383.8 139.5 all-gather.11
  526.0 180.2 all-gather.13
  720.4 8.8 reduce-scatter.4
where the time goes:
time: 743 us; the launch traced here: 741 us
  waiting for transfers between devices  612 us (82%)
  matrix products  55.5 us (7%)
  other arithmetic  27.8 us (4%)
  local copies, waits for them, and re-layouts  26 us (3%)
  between operations  13.6 us (2%)
    all_gather x1, waiting for transfers between devices, local(): lax.all_gather(down_weight, 'sp', axis=1, tiled=True)  183 us
    all_gather x1, waiting for transfers between devices, local(): lax.all_gather(gate_weight, 'sp', axis=0, tiled=True)  138 us
    all_gather x1, waiting for transfers between devices, local(): lax.all_gather(up_weight, 'sp', axis=0, tiled=True)  134 us
    all_gather x1, waiting for transfers between devices, local(): value_rows = lax.all_gather(values, 'sp', axis=0, tiled=True)  69.2 us
    all_gather x1, waiting for transfers between devices, local(): key_rows = lax.all_gather(keys, 'sp', axis=0, tiled=True)  68.9 us
    convert_element_type x4, other arithmetic, update(): expo.astype(jnp.bfloat16)  17.4 us
    dot_general x4, matrix products, update(): jnp.einsum('qhcd,khcd->chqk', query_four, key_part, preferred_element_typ...  16.9 us
  transfers between devices with their start and end apart: 7, of which 7 were waited for; matrix products, arithmetic and copies ran while one was open for 1% of the time, Pallas kernels for 0%

commit v1 on v0

--- a/solution.py
+++ b/solution.py
@@ -1,10 +1,16 @@
+import functools
+
 import jax
 import jax.numpy as jnp
 from jax import lax
+from jax.experimental import pallas as pl
+from jax.experimental.pallas import tpu as pltpu
 from jax.sharding import PartitionSpec as P
 
 QK = 64
 VD = 128
+LANE = 128
+VMEM_LIMIT = 60 * 1024 * 1024
 
 
 def rms_rows(first, norm_gain):
@@ -13,7 +19,7 @@
     ).astype(jnp.bfloat16)
 
 
-def local(
+def generic(
     resid,
     queries,
     keys,
@@ -33,7 +39,6 @@
     query_four = queries.reshape(tok_rows, local_heads, 2, QK)
     score_scale = QK ** (-0.5)
     query_pos = offset + lax.iota(jnp.int32, tok_rows)
-    last_query = offset + tok_rows - 1
 
     def update(fold_state, key_part, value_part, key_pos):
         run_max, run_sum, run_acc = fold_state
@@ -78,15 +83,7 @@
         key_pos = span_start + lax.iota(jnp.int32, key_span)
         return update(inner_state, key_part, value_part, key_pos)
 
-    def run_spans(inner_state):
-        return lax.fori_loop(0, key_count // key_span, one_span, inner_state)
-
-    def keep_state(inner_state):
-        return inner_state
-
-    final_max, final_sum, final_acc = lax.cond(
-        jnp.int32(0) <= last_query, run_spans, keep_state, initial
-    )
+    final_max, final_sum, final_acc = lax.fori_loop(0, key_count // key_span, one_span, initial)
     ratio = final_acc / final_sum[..., None]
     mixed_heads = ratio[0] - lambdas[:, None, None] * ratio[1]
     head_out = (
@@ -130,7 +127,495 @@
     return lax.all_gather(finished, "tp", axis=0, tiled=True)
 
 
+def where_am_i(R):
+    s = lax.axis_index("sp")
+    return s // R, lax.rem(s, R), lax.axis_index("tp")
+
+
+def remote(src, dst, send, recv, sp, tp):
+    return pltpu.make_async_remote_copy(
+        src_ref=src,
+        dst_ref=dst,
+        send_sem=send,
+        recv_sem=recv,
+        device_id={"sp": sp, "tp": tp},
+        device_id_type=pl.DeviceIdType.MESH,
+    )
+
+
+def greet(peers):
+    barrier = pltpu.get_barrier_semaphore()
+    for sp, tp in peers:
+        pl.semaphore_signal(
+            barrier,
+            inc=1,
+            device_id={"sp": sp, "tp": tp},
+            device_id_type=pl.DeviceIdType.MESH,
+        )
+    pl.semaphore_wait(barrier, len(peers))
+
+
+def first_block(zz, share):
+    return (zz * share) // LANE
+
+
+def mirror_x(r):
+    return r + 1 - 2 * lax.rem(r, 2)
+
+
+def mirror_y(r):
+    return r + 2 - 4 * (lax.rem(r, 4) // 2)
+
+
+def gather_kernel(Z, R, share, width, ins, outs, sems):
+    q_in, k_in, v_in, g_in, u_in, d_in = ins
+    q_out, k_out, v_out, g_out, u_out, d_out = outs
+    send1, recv1, send2, recv2, local_sem = sems
+    z, r, t = where_am_i(R)
+    rx, ry = mirror_x(r), mirror_y(r)
+    rd = mirror_x(ry)
+    T = k_in.shape[0]
+    W = g_in.shape[0]
+
+    def dev(zz, rr):
+        return zz * R + rr
+
+    greet([(dev(lax.rem(z + j, Z), r), t) for j in range(1, Z)] + [(dev(z, rx), t), (dev(z, ry), t)])
+
+    def cols(zz):
+        return pl.ds(pl.multiple_of(zz * VD, LANE), VD)
+
+    def wide(zz):
+        return pl.ds(pl.multiple_of(first_block(zz, share) * LANE, LANE), width)
+
+    def source(a, zz, h=None):
+        ref = (q_in, k_in, v_in, g_in, u_in, d_in)[a]
+        if a == 5:
+            start = pl.multiple_of(first_block(zz, share) * LANE, LANE)
+            if h is None:
+                return ref.at[pl.ds(start, width), :]
+            n = width // 2
+            return ref.at[pl.ds(pl.multiple_of(start + h * n, 64), n), :]
+        rows = T if a < 3 else W
+        sl = cols(zz) if a < 3 else wide(zz)
+        if h is None:
+            return ref.at[:, sl]
+        n = rows // 2
+        return ref.at[pl.ds(h * n, n), sl]
+
+    def place(a, zz, rr, h=None):
+        ref = (q_out, k_out, v_out, g_out, u_out, d_out)[a]
+        if a == 0:
+            return ref.at[zz]
+        slot = dev(zz, rr)
+        if h is None:
+            return ref.at[slot]
+        n = ref.shape[1] // 2
+        return ref.at[slot, pl.ds(h * n, n), :]
+
+    def first_hop(a, j):
+        zz = lax.rem(z + j, Z)
+        return remote(source(a, zz), place(a, z, r), send1.at[a, j], recv1.at[a, j], dev(zz, r), t)
+
+    def arrived(a, j):
+        zz = lax.rem(z + Z - j, Z)
+        remote(source(a, z), place(a, zz, r), send1.at[a, j], recv1.at[a, j], dev(zz, r), t).wait_recv()
+
+    started = []
+    locals_ = []
+    for group in ((1, 2, 0), (3, 4, 5)):
+        for j in range(1, Z):
+            for a in group:
+                c = first_hop(a, j)
+                c.start()
+                started.append(c)
+        for a in group:
+            c = pltpu.make_async_copy(source(a, z), place(a, z, r), local_sem.at[a])
+            c.start()
+            locals_.append(c)
+
+    def hop2(a, j, kind, owner, h, target, from_input):
+        zz = lax.rem(z + Z - j, Z)
+        src = source(a, z, h) if from_input else place(a, zz, owner, h)
+        return remote(
+            src,
+            place(a, zz, owner, h),
+            send2.at[a - 1, j, kind],
+            recv2.at[a - 1, j, kind],
+            dev(z, target),
+            t,
+        )
+
+    def wait2(a, j, kind):
+        owner = (rx, rx, ry, ry, rd, rd)[kind]
+        h = (0, 1, 0, 1, 0, 1)[kind]
+        target = (rx, rx, ry, ry, ry, rx)[kind]
+        hop2(a, j, kind, owner, h, target, False).wait_recv()
+
+    pieces = [(a, j) for j in range(Z) for a in (1, 2)] + [
+        (a, j) for j in range(Z) for a in (3, 4, 5)
+    ]
+    lag = 2
+    for i in range(len(pieces) + lag):
+        if i < len(pieces):
+            a, j = pieces[i]
+            if j:
+                arrived(a, j)
+            for kind, h, target in ((0, 0, rx), (3, 1, ry), (1, 1, rx), (2, 0, ry)):
+                c = hop2(a, j, kind, r, h, target, j == 0)
+                c.start()
+                started.append(c)
+        if i >= lag:
+            a, j = pieces[i - lag]
+            wait2(a, j, 0)
+            c = hop2(a, j, 4, rx, 0, ry, False)
+            c.start()
+            started.append(c)
+            wait2(a, j, 3)
+            c = hop2(a, j, 5, ry, 1, rx, False)
+            c.start()
+            started.append(c)
+    for a, j in pieces:
+        for kind in (1, 2, 4, 5):
+            wait2(a, j, kind)
+    for j in range(1, Z):
+        arrived(0, j)
+    for c in locals_:
+        c.wait()
+    for c in started:
+        c.wait_send()
+
+
+def gather_all(Z, R, q, k, v, g, u, d):
+    T, W = k.shape[0], g.shape[0]
+    share = g.shape[1] // Z
+    width = max(
+        -(-((zz + 1) * share) // LANE) - (zz * share) // LANE for zz in range(Z)
+    ) * LANE
+    S = Z * R
+
+    def kernel(*refs):
+        gather_kernel(Z, R, share, width, refs[:6], refs[6:12], refs[12:])
+
+    bf = jnp.bfloat16
+    return pl.pallas_call(
+        kernel,
+        out_shape=[
+            jax.ShapeDtypeStruct((Z, T, VD), bf),
+            jax.ShapeDtypeStruct((S, T, VD), bf),
+            jax.ShapeDtypeStruct((S, T, VD), bf),
+            jax.ShapeDtypeStruct((S, W, width), bf),
+            jax.ShapeDtypeStruct((S, W, width), bf),
+            jax.ShapeDtypeStruct((S, width, d.shape[1]), bf),
+        ],
+        in_specs=[pl.BlockSpec(memory_space=pltpu.VMEM)] * 6,
+        out_specs=[pl.BlockSpec(memory_space=pl.ANY)] * 6,
+        scratch_shapes=[
+            pltpu.SemaphoreType.DMA((6, Z)),
+            pltpu.SemaphoreType.DMA((6, Z)),
+            pltpu.SemaphoreType.DMA((5, Z, 6)),
+            pltpu.SemaphoreType.DMA((5, Z, 6)),
+            pltpu.SemaphoreType.DMA((6,)),
+        ],
+        compiler_params=pltpu.CompilerParams(
+            collective_id=0, has_side_effects=True, vmem_limit_bytes=VMEM_LIMIT
+        ),
+    )(q, k, v, g, u, d)
+
+
+def attention_block(R, T, i, r, q_at, k_at, v_at, lam, gain):
+    span = R * T
+    query = q_at(i) * jnp.bfloat16(QK**-0.5)
+    ratios = []
+    for c in range(2):
+        part = query[:, c * QK : (c + 1) * QK]
+
+        def fold(n, state, masked):
+            run_max, run_sum, run_acc = state
+            key = k_at(n)[:, c * QK : (c + 1) * QK]
+            scores = lax.dot_general(
+                part, key, (((1,), (1,)), ((), ())), preferred_element_type=jnp.float32
+            )
+            if masked:
+                qpos = r * T + lax.broadcasted_iota(jnp.int32, scores.shape, 0)
+                kpos = lax.broadcasted_iota(jnp.int32, scores.shape, 1)
+                scores = jnp.where(kpos <= qpos, scores, -1e30)
+            new_max = jnp.maximum(run_max, jnp.max(scores, axis=-1, keepdims=True))
+            expo = jnp.exp(scores - new_max)
+            factor = jnp.exp(run_max - new_max)
+            new_sum = run_sum * factor + jnp.sum(expo, axis=-1, keepdims=True)
+            new_acc = run_acc * factor + jnp.dot(
+                expo.astype(jnp.bfloat16), v_at(n), preferred_element_type=jnp.float32
+            )
+            return new_max, new_sum, new_acc
+
+        state = (
+            jnp.full((T, 1), -1e30, jnp.float32),
+            jnp.zeros((T, 1), jnp.float32),
+            jnp.zeros((T, VD), jnp.float32),
+        )
+        state = fold(i, state, True)
+        state = lax.fori_loop(0, i, lambda n, st: fold(n, st, False), state)
+        ratios.append(state[2] / state[1])
+    mixed = ratios[0] - lam * ratios[1]
+    return (
+        mixed * lax.rsqrt(jnp.mean(mixed * mixed, axis=-1, keepdims=True) + 1e-05) * gain
+    ).astype(jnp.bfloat16)
+
+
+def attention_kernel(Z, R, q_ref, k_ref, v_ref, lam_ref, gain_ref, out_ref):
+    z, r, _ = where_am_i(R)
+    T = q_ref.shape[1]
+    span = R * T
+    lam = lam_ref[z]
+
+    def at(ref, n):
+        return ref[pl.ds(pl.multiple_of(n * span, span), span), :]
+
+    @pl.loop(0, Z)
+    def _(i):
+        out_ref[i] = attention_block(
+            R,
+            T,
+            i,
+            r,
+            lambda b: q_ref[b],
+            lambda n: at(k_ref, n),
+            lambda n: at(v_ref, n),
+            lam,
+            gain_ref[...],
+        )
+
+
+def attention(Z, R, q, k, v, lambdas, head_gain):
+    vm = pl.BlockSpec(memory_space=pltpu.VMEM)
+    return pl.pallas_call(
+        functools.partial(attention_kernel, Z, R),
+        out_shape=jax.ShapeDtypeStruct(q.shape, jnp.bfloat16),
+        in_specs=[vm, vm, vm, pl.BlockSpec(memory_space=pltpu.SMEM), vm],
+        out_specs=vm,
+        compiler_params=pltpu.CompilerParams(vmem_limit_bytes=VMEM_LIMIT),
+    )(q, k, v, lambdas, head_gain.reshape(1, -1))
+
+
+def branch_kernel(
+    Z, R, ho, resid, w, gain, first_ref, all_ref, heads, part, got, norm_sc, sem_a, sem_b, sem_c, sem_d, loc
+):
+    z, r, t = where_am_i(R)
+    me = z * R + r
+    T = resid.shape[0]
+    H = T // 2
+    greet([(lax.rem(z + j, Z) * R + r, t) for j in range(1, Z)] + [(me, 1 - t)])
+    copies = []
+    for j in range(1, Z):
+        zz = lax.rem(z + j, Z)
+        c = remote(ho.at[zz], heads.at[z], sem_a.at[0, j], sem_a.at[1, j], zz * R + r, t)
+        c.start()
+        copies.append(c)
+    own = pltpu.make_async_copy(ho.at[z], heads.at[z], loc.at[0])
+    own.start()
+    own.wait()
+    for c in copies:
+        c.wait()
+    D = w.shape[1]
+    NT = 512 if D % 512 == 0 else D
+    for h in range(2):
+        hh = (1 - t) if h == 0 else t
+        rows = pl.ds(pl.multiple_of(hh * H, 16), H)
+        left = jnp.concatenate([heads[n, rows, :] for n in range(Z)], axis=1)
+        for n in range(0, D, NT):
+            part[h, :, n : n + NT] = jnp.dot(
+                left, w[:, n : n + NT], preferred_element_type=jnp.float32
+            ).astype(jnp.bfloat16)
+        if h == 0:
+            swap = remote(part.at[0], got, sem_b.at[0], sem_b.at[1], me, 1 - t)
+            swap.start()
+    swap.wait()
+    own_rows = pl.ds(pl.multiple_of(t * H, 16), H)
+    first = resid[own_rows, :].astype(jnp.float32) + (
+        part[1].astype(jnp.float32) + got[...].astype(jnp.float32)
+    )
+    first_ref[...] = first
+    norm_sc[...] = rms_rows(first, gain[...])
+
+    def rows_of(zz, tt):
+        return all_ref.at[pl.ds(pl.multiple_of(zz * T + tt * H, 16), H), :]
+
+    copies = []
+    for j in range(1, Z):
+        zz = lax.rem(z + j, Z)
+        c = remote(norm_sc, rows_of(z, t), sem_c.at[0, j], sem_c.at[1, j], zz * R + r, t)
+        c.start()
+        copies.append(c)
+    across = [remote(norm_sc, rows_of(z, t), sem_d.at[0, 0], sem_d.at[1, 0], me, 1 - t)]
+    across[0].start()
+    own = pltpu.make_async_copy(norm_sc, rows_of(z, t), loc.at[1])
+    own.start()
+    for j in range(1, Z):
+        zz = lax.rem(z + Z - j, Z)
+        remote(norm_sc, rows_of(zz, t), sem_c.at[0, j], sem_c.at[1, j], zz * R + r, t).wait_recv()
+        c = remote(rows_of(zz, t), rows_of(zz, t), sem_d.at[0, j], sem_d.at[1, j], me, 1 - t)
+        c.start()
+        across.append(c)
+    own.wait()
+    for c in copies:
+        c.wait_send()
+    for j in range(Z):
+        zz = lax.rem(z + Z - j, Z)
+        remote(
+            rows_of(zz, t), rows_of(zz, 1 - t), sem_d.at[0, j], sem_d.at[1, j], me, 1 - t
+        ).wait_recv()
+    for c in across:
+        c.wait_send()
+
+
+def branch(Z, R, ho, resid, w, norm_gain):
+    vm = pl.BlockSpec(memory_space=pltpu.VMEM)
+    T, D = resid.shape
+    H = T // 2
+    return pl.pallas_call(
+        functools.partial(branch_kernel, Z, R),
+        out_shape=[
+            jax.ShapeDtypeStruct((H, D), jnp.float32),
+            jax.ShapeDtypeStruct((Z * T, D), jnp.bfloat16),
+        ],
+        in_specs=[vm] * 4,
+        out_specs=[vm, vm],
+        scratch_shapes=[
+            pltpu.VMEM(ho.shape, jnp.bfloat16),
+            pltpu.VMEM((2, H, D), jnp.bfloat16),
+            pltpu.VMEM((H, D), jnp.bfloat16),
+            pltpu.VMEM((H, D), jnp.bfloat16),
+            pltpu.SemaphoreType.DMA((2, Z)),
+            pltpu.SemaphoreType.DMA((2,)),
+            pltpu.SemaphoreType.DMA((2, Z)),
+            pltpu.SemaphoreType.DMA((2, Z)),
+            pltpu.SemaphoreType.DMA((2,)),
+        ],
+        compiler_params=pltpu.CompilerParams(
+            collective_id=1, has_side_effects=True, vmem_limit_bytes=VMEM_LIMIT
+        ),
+    )(ho, resid, w, norm_gain.reshape(1, -1))
+
+
+def finish_kernel(Z, R, terms, first, out, cross, sums, landed, mine, sem_a, sem_b, sem_c, loc):
+    z, r, t = where_am_i(R)
+    me = z * R + r
+    H = first.shape[0]
+    greet([(lax.rem(z + j, Z) * R + r, t) for j in range(1, Z)] + [(me, 1 - t)])
+    copies = []
+    order = [j % Z for j in range(1, Z + 1)]
+    for j in order:
+        zz = lax.rem(z + j, Z)
+        c = remote(
+            terms.at[zz, 1 - t], cross.at[zz], sem_a.at[0, j], sem_a.at[1, j], me, 1 - t
+        )
+        c.start()
+        copies.append(c)
+    sent = []
+    total = None
+    for n, j in enumerate(order):
+        zz = lax.rem(z + j, Z)
+        copies[n].wait()
+        total = terms[zz, t].astype(jnp.float32) + cross[zz].astype(jnp.float32)
+        if j:
+            sums[j] = total.astype(jnp.bfloat16)
+            c = remote(sums.at[j], landed.at[j], sem_b.at[0, j], sem_b.at[1, j], zz * R + r, t)
+            c.start()
+            sent.append(c)
+        else:
+            mine[...] = total
+    for c in sent:
+        c.wait()
+    total = mine[...]
+    for j in range(1, Z):
+        total = total + landed[j].astype(jnp.float32)
+    rows = pl.ds(pl.multiple_of(t * H, 16), H)
+    sums[0] = (first[...] + 0.5 * total).astype(jnp.bfloat16)
+    c = remote(sums.at[0], out.at[rows, :], sem_c.at[0], sem_c.at[1], me, 1 - t)
+    c.start()
+    own = pltpu.make_async_copy(sums.at[0], out.at[rows, :], loc)
+    own.start()
+    own.wait()
+    c.wait()
+
+
+def finish(Z, R, terms, first):
+    vm = pl.BlockSpec(memory_space=pltpu.VMEM)
+    H, D = first.shape
+    return pl.pallas_call(
+        functools.partial(finish_kernel, Z, R),
+        out_shape=jax.ShapeDtypeStruct((2 * H, D), jnp.bfloat16),
+        in_specs=[vm, vm],
+        out_specs=vm,
+        scratch_shapes=[
+            pltpu.VMEM((Z, H, D), jnp.bfloat16),
+            pltpu.VMEM((Z, H, D), jnp.bfloat16),
+            pltpu.VMEM((Z, H, D), jnp.bfloat16),
+            pltpu.VMEM((H, D), jnp.float32),
+            pltpu.SemaphoreType.DMA((2, Z)),
+            pltpu.SemaphoreType.DMA((2, Z)),
+            pltpu.SemaphoreType.DMA((2,)),
+            pltpu.SemaphoreType.DMA,
+        ],
+        compiler_params=pltpu.CompilerParams(
+            collective_id=2, has_side_effects=True, vmem_limit_bytes=VMEM_LIMIT
+        ),
+    )(terms, first)
+
+
+def columns_form(
+    resid,
+    queries,
+    keys,
+    values,
+    lambdas,
+    head_gain,
+    out_weight,
+    norm_gain,
+    gate_weight,
+    up_weight,
+    down_weight,
+):
+    Z = lambdas.shape[0]
+    R = lax.axis_size("sp") // Z
+    T, D = resid.shape
+    share = gate_weight.shape[1] // Z
+    q, k, v, g, u, d = gather_all(Z, R, queries, keys, values, gate_weight, up_weight, down_weight)
+    S = Z * R
+    ho = attention(
+        Z, R, q, k.reshape(S * T, VD), v.reshape(S * T, VD), lambdas, head_gain
+    )
+    first, normed = branch(Z, R, ho, resid, out_weight, norm_gain)
+    width = g.shape[2]
+    gate = jnp.dot(normed, g.reshape(D, width), preferred_element_type=jnp.float32)
+    up = jnp.dot(normed, u.reshape(D, width), preferred_element_type=jnp.float32)
+    z = lax.axis_index("sp") // R
+    unit = first_block(z, share) * LANE + lax.iota(jnp.int32, width)
+    counted = (unit >= z * share) & (unit < (z + 1) * share)
+    hidden = jnp.where(counted[None, :], jax.nn.silu(gate) * up, 0.0).astype(jnp.bfloat16)
+    terms = jnp.dot(
+        hidden, jnp.transpose(d, (1, 0, 2)).reshape(width, D), preferred_element_type=jnp.float32
+    ).astype(jnp.bfloat16)
+    return finish(Z, R, terms.reshape(Z, 2, T // 2, D), first)
+
+
 def solution(mesh):
+    sp, tp = mesh.shape["sp"], mesh.shape["tp"]
+
+    def local(*args):
+        heads = args[4].shape[0]
+        tok_rows = args[1].shape[0]
+        columns = (
+            tp == 2
+            and heads > 1
+            and sp == 4 * heads
+            and args[10].shape[1] % LANE == 0
+            and args[8].shape[1] % (16 * heads) == 0
+            and tok_rows % 32 == 0
+        )
+        return (columns_form if columns else generic)(*args)
+
     return jax.shard_map(
         local,
         mesh=mesh,

time: 743 us -> 260 us (0.35)
  waiting for transfers between devices: 612 us -> 0 us
  Pallas kernels: 0 us -> 234 us
  matrix products: 55.5 us -> 17.9 us
  other arithmetic: 27.8 us -> 0.01 us
  local copies, waits for them, and re-layouts: 26 us -> 5.27 us
  between operations: 13.6 us -> 0.04 us
    all_gather x5 -> x0, waiting for transfers between devices: 593 us -> none  [the longest x1 183 us: local(): lax.all_gather(down_weight, 'sp', axis=1, tiled=True)]
    pallas_call x0 -> x4, Pallas kernels: none -> 234 us  [the longest x1 105 us: gather_all(): pl.pallas_call(kernel, out_shape=[jax.ShapeDtypeStruct((Z, T, VD), bf), j...]
    dot_general x11 -> x2, matrix products: 55.5 us -> 17.9 us  [the longest x1 11 us: columns_form(): jnp.dot(hidden, jnp.transpose(d, (1, 0, 2)).reshape(width, D), preferred_...]
    dynamic_slice x12 -> x0, local copies, waits for them, and re-layouts: 23.3 us -> none  [the longest x8 14.2 us: one_span(): lax.dynamic_slice_in_dim(value_rows, span_start, key_span, 0)]
    convert_element_type x6 -> x0, other arithmetic: 19.7 us -> none  [the longest x4 17.4 us: update(): expo.astype(jnp.bfloat16)]
    reduce_scatter x2 -> x0, waiting for transfers between devices: 16.9 us -> none  [the longest x1 9.04 us: local(): lax.psum_scatter(terms.astype(jnp.bfloat16), 'tp', scatter_dimension=0, t...]
  transfers between devices with their start and end apart: 7 -> 0, of which waited for: 7 -> 0; matrix products, arithmetic and copies ran while one was open for 1% -> 0% of each run, Pallas kernels for 0% -> 0%
where the time goes in v1:
time: 260 us; the launch traced here: 257 us
  Pallas kernels  234 us (90%)
  matrix products  17.9 us (7%)
  local copies, waits for them, and re-layouts  5.27 us (2%)
    pallas_call x1, Pallas kernels, gather_all(): pl.pallas_call(kernel, out_shape=[jax.ShapeDtypeStruct((Z, T, VD), bf), j...  105 us
    pallas_call x1, Pallas kernels, branch(): pl.pallas_call(functools.partial(branch_kernel, Z, R), out_shape=[jax.Sha...  70 us
    pallas_call x1, Pallas kernels, finish(): pl.pallas_call(functools.partial(finish_kernel, Z, R), out_shape=jax.Shap...  44 us
    pallas_call x1, Pallas kernels, attention(): pl.pallas_call(functools.partial(attention_kernel, Z, R), out_shape=jax.S...  15 us
    dot_general x1, matrix products, columns_form(): jnp.dot(hidden, jnp.transpose(d, (1, 0, 2)).reshape(width, D), preferred_...  11 us
    dot_general x1, matrix products, columns_form(): jnp.dot(normed, g.reshape(D, width), preferred_element_type=jnp.float32)  6.85 us

profile of v1, /device:TPU:25, one launch (start us, length us, event | category | flops | bytes accessed | tf_op | source)
XLA Modules:
  0.0 257.0 jit_solution(5937351719462715121)
XLA Ops:
  0.0 104.9 %shard_map.109 = (bf16[4,192,128]{2,1,0:T(8,128)(2,1)}, bf16[16,192,128]{2,1,0:T(8,128)(2,1)}, bf16[16,192,128]{2,1,0:T(8,128)(2,1)}, bf16[16,128,768]{2,1,0:T(8...) custom-call(bf16[192,512]{1,0:T(8,128)(2,1)} %refs_0_.1, bf16[192,512]{1,0:T(8,128)(2,1)} %refs_1_.1, ...), custom_call_target="tpu_custom_call" | custom-call | tf_op jit(solution)/shard_map/pallas_call | solution.py:301
  104.9 15.0 %shard_map.110.ho = bf16[4,192,128]{2,1,0:T(8,128)(2,1)} custom-call(bf16[4,192,128]{2,1,0:T(8,128)(2,1)} %get-tuple-element.13.q_ref, bf16[3072,128]{1,0:T(8,128)(2,1)} %bitcast.17, bf16[3072,128]{1,0:T(8,128)(2,1)} %bitcast.18, f32[4]{0:T(128)} %lam_ref.1, f32[1,128]{1,0:T(1,128)} %bitcast.20), custom_call_target="tpu_custom_call" | custom-call | tf_op jit(solution)/shard_map/pallas_call | solution.py:392
  119.8 3.2 %copy.12 = bf16[768,16,128]{0,2,1:T(8,128)(2,1)S(1)} copy(bf16[768,16,128]{2,0,1:T(8,128)(2,1)} %bitcast.15) | data formatting | bytes 6291456 | tf_op jit(solution)/shard_map/transpose | solution.py:598
  123.0 70.0 %shard_map.111 = (f32[96,2048]{1,0:T(8,128)}, bf16[768,2048]{1,0:T(8,128)(2,1)}) custom-call(bf16[4,192,128]{2,1,0:T(8,128)(2,1)} %shard_map.110.ho, bf16[192,2048]{1,0:T(8,128)(2,1)} %resid.1, bf16[512,2048]{1,0:T(8,128)(2,1)} %w.1, f32[1,2048]{1,0:T(1,128)} %bitcast.19), custom_call_target="tpu_custom_call" | custom-call | tf_op jit(solution)/shard_map/pallas_call | solution.py:476
  193.0 6.8 %fusion.5 = f32[768,768]{1,0:T(8,128)} fusion(bf16[768,2048]{1,0:T(8,128)(2,1)} %get-tuple-element.16, bf16[2048,768]{1,0:T(8,128)(2,1)} %bitcast.22), kind=kOutput, calls=%fused_computation.8 | convolution fusion | flops 2415919104 | bytes 8650752 | tf_op jit(solution)/shard_map/dot_general | solution.py:591
  199.9 11.0 %convolution_convert_fusion = bf16[768,2048]{1,0:T(8,128)(2,1)} fusion(bf16[768,2048]{0,1:T(8,128)(2,1)S(1)} %bitcast.14, f32[768,768]{1,0:T(8,128)} %fusion.5, bf16[768,2048]{1,0:T(8,128)(2,1)} %get-tuple-element.16, bf16[2048,768]{1,0:T(8,128)(2,1)} %bitcast.21, pred[768]{0:T(1024)(128)(4,1)S(1)} %fusion.2), kind=kOutput, calls=%fused_computation | convolution fusion | flops 4837539840 | bytes 14942976 | tf_op jit(solution)/shard_map/dot_general | solution.py:597
  210.9 44.0 %shard_map.112 = bf16[192,2048]{1,0:T(8,128)(2,1)} custom-call(bf16[4,2,96,2048]{3,2,1,0:T(8,128)(2,1)} %bitcast.16, f32[96,2048]{1,0:T(8,128)} %get-tuple-element.20.first), custom_call_target="tpu_custom_call" | custom-call | tf_op jit(solution)/shard_map/pallas_call | solution.py:546
  254.9 2.1 copy.14
  (1 shorter events, 0.0 us)

commit v2 on v0

--- a/solution.py
+++ b/solution.py
@@ -1,10 +1,14 @@
 import jax
 import jax.numpy as jnp
 from jax import lax
+from jax.experimental import pallas as pl
+from jax.experimental.pallas import tpu as pltpu
 from jax.sharding import PartitionSpec as P
 
 QK = 64
 VD = 128
+LANE = 128
+VMEM_LIMIT = 60 * 1024 * 1024
 
 
 def rms_rows(first, norm_gain):
@@ -13,7 +17,7 @@
     ).astype(jnp.bfloat16)
 
 
-def local(
+def generic(
     resid,
     queries,
     keys,
@@ -33,7 +37,6 @@
     query_four = queries.reshape(tok_rows, local_heads, 2, QK)
     score_scale = QK ** (-0.5)
     query_pos = offset + lax.iota(jnp.int32, tok_rows)
-    last_query = offset + tok_rows - 1
 
     def update(fold_state, key_part, value_part, key_pos):
         run_max, run_sum, run_acc = fold_state
@@ -78,15 +81,7 @@
         key_pos = span_start + lax.iota(jnp.int32, key_span)
         return update(inner_state, key_part, value_part, key_pos)
 
-    def run_spans(inner_state):
-        return lax.fori_loop(0, key_count // key_span, one_span, inner_state)
-
-    def keep_state(inner_state):
-        return inner_state
-
-    final_max, final_sum, final_acc = lax.cond(
-        jnp.int32(0) <= last_query, run_spans, keep_state, initial
-    )
+    final_max, final_sum, final_acc = lax.fori_loop(0, key_count // key_span, one_span, initial)
     ratio = final_acc / final_sum[..., None]
     mixed_heads = ratio[0] - lambdas[:, None, None] * ratio[1]
     head_out = (
@@ -130,7 +125,498 @@
     return lax.all_gather(finished, "tp", axis=0, tiled=True)
 
 
+def where_am_i(R):
+    s = lax.axis_index("sp")
+    return s // R, lax.rem(s, R), lax.axis_index("tp")
+
+
+def remote(src, dst, send, recv, sp, tp):
+    return pltpu.make_async_remote_copy(
+        src_ref=src,
+        dst_ref=dst,
+        send_sem=send,
+        recv_sem=recv,
+        device_id={"sp": sp, "tp": tp},
+        device_id_type=pl.DeviceIdType.MESH,
+    )
+
+
+def greet(peers):
+    barrier = pltpu.get_barrier_semaphore()
+    for sp, tp in peers:
+        pl.semaphore_signal(
+            barrier,
+            inc=1,
+            device_id={"sp": sp, "tp": tp},
+            device_id_type=pl.DeviceIdType.MESH,
+        )
+    pl.semaphore_wait(barrier, len(peers))
+
+
+def first_block(zz, share):
+    return (zz * share) // LANE
+
+
+def mirror_x(r):
+    return r + 1 - 2 * lax.rem(r, 2)
+
+
+def mirror_y(r):
+    return r + 2 - 4 * (lax.rem(r, 4) // 2)
+
+
+def attention_block(R, T, i, r, q_at, k_at, v_at, lam, gain):
+    span = R * T
+    query = q_at(i) * jnp.bfloat16(QK**-0.5)
+    ratios = []
+    for c in range(2):
+        part = query[:, c * QK : (c + 1) * QK]
+
+        def fold(n, state, masked):
+            run_max, run_sum, run_acc = state
+            key = k_at(n)[:, c * QK : (c + 1) * QK]
+            scores = lax.dot_general(
+                part, key, (((1,), (1,)), ((), ())), preferred_element_type=jnp.float32
+            )
+            if masked:
+                qpos = r * T + lax.broadcasted_iota(jnp.int32, scores.shape, 0)
+                kpos = lax.broadcasted_iota(jnp.int32, scores.shape, 1)
+                scores = jnp.where(kpos <= qpos, scores, -1e30)
+            new_max = jnp.maximum(run_max, jnp.max(scores, axis=-1, keepdims=True))
+            expo = jnp.exp(scores - new_max)
+            factor = jnp.exp(run_max - new_max)
+            new_sum = run_sum * factor + jnp.sum(expo, axis=-1, keepdims=True)
+            new_acc = run_acc * factor + jnp.dot(
+                expo.astype(jnp.bfloat16), v_at(n), preferred_element_type=jnp.float32
+            )
+            return new_max, new_sum, new_acc
+
+        state = (
+            jnp.full((T, 1), -1e30, jnp.float32),
+            jnp.zeros((T, 1), jnp.float32),
+            jnp.zeros((T, VD), jnp.float32),
+        )
+        state = fold(i, state, True)
+        state = lax.fori_loop(0, i, lambda n, st: fold(n, st, False), state)
+        ratios.append(state[2] / state[1])
+    mixed = ratios[0] - lam * ratios[1]
+    return (
+        mixed * lax.rsqrt(jnp.mean(mixed * mixed, axis=-1, keepdims=True) + 1e-05) * gain
+    ).astype(jnp.bfloat16)
+
+
+def whole_kernel(Z, R, share, width, refs):
+    (
+        q_in, k_in, v_in, g_in, u_in, d_in, resid_in, w_in, lam, head_gain, norm_gain,
+        out,
+        q_sc, k_sc, v_sc, g_sc, u_sc, d_sc, resid, w,
+        ho, heads, part, got, first, norm_sc, all_sc,
+        hidden, terms, cross, sums, landed,
+        send1, recv1, send2, recv2, local_sem, ho_sem, swap_sem, ag_sem, core_sem,
+        cross_sem, sum_sem, out_sem,
+    ) = refs
+    ins = (q_in, k_in, v_in, g_in, u_in, d_in)
+    outs = (q_sc, k_sc, v_sc, g_sc, u_sc, d_sc)
+    z, r, t = where_am_i(R)
+    me = z * R + r
+    rx, ry = mirror_x(r), mirror_y(r)
+    rd = mirror_x(ry)
+    T = k_in.shape[0]
+    W = g_in.shape[0]
+    D = resid_in.shape[1]
+    H = T // 2
+    ahead = [lax.rem(z + j, Z) for j in range(Z)]
+    behind = [lax.rem(z + Z - j, Z) for j in range(Z)]
+
+    def dev(zz, rr):
+        return zz * R + rr
+
+    greet(
+        [(dev(ahead[j], r), t) for j in range(1, Z)]
+        + [(dev(z, rx), t), (dev(z, ry), t), (me, 1 - t)]
+    )
+
+    def source(a, zz, h=None):
+        ref = ins[a]
+        if a == 5:
+            start = pl.multiple_of(first_block(zz, share) * LANE, LANE)
+            if h is None:
+                return ref.at[pl.ds(start, width), :]
+            n = width // 2
+            return ref.at[pl.ds(pl.multiple_of(start + h * n, 64), n), :]
+        if a < 3:
+            rows, sl = T, pl.ds(pl.multiple_of(zz * VD, LANE), VD)
+        else:
+            rows, sl = W, pl.ds(pl.multiple_of(first_block(zz, share) * LANE, LANE), width)
+        if h is None:
+            return ref.at[:, sl]
+        n = rows // 2
+        return ref.at[pl.ds(h * n, n), sl]
+
+    def place(a, zz, rr, h=None):
+        ref = outs[a]
+        if a == 0:
+            return ref.at[zz]
+        slot = dev(zz, rr)
+        if h is None:
+            return ref.at[slot]
+        n = ref.shape[1] // 2
+        return ref.at[slot, pl.ds(h * n, n), :]
+
+    started, locals_ = [], []
+
+    def first_hop(a, j):
+        c = remote(
+            source(a, ahead[j]), place(a, z, r), send1.at[a, j], recv1.at[a, j], dev(ahead[j], r), t
+        )
+        c.start()
+        started.append(c)
+
+    def arrived(a, j):
+        zz = behind[j]
+        remote(
+            source(a, z), place(a, zz, r), send1.at[a, j], recv1.at[a, j], dev(zz, r), t
+        ).wait_recv()
+
+    def keep(src, dst, n):
+        c = pltpu.make_async_copy(src, dst, local_sem.at[n])
+        c.start()
+        locals_.append(c)
+
+    def hop2(a, j, kind, owner, h, target, from_input):
+        zz = behind[j]
+        src = source(a, z, h) if from_input else place(a, zz, owner, h)
+        return remote(
+            src,
+            place(a, zz, owner, h),
+            send2.at[a - 1, j, kind],
+            recv2.at[a - 1, j, kind],
+            dev(z, target),
+            t,
+        )
+
+    def wait2(a, j, kind):
+        owner = (rx, rx, ry, ry, rd, rd)[kind]
+        target = (rx, rx, ry, ry, ry, rx)[kind]
+        hop2(a, j, kind, owner, kind % 2, target, False).wait_recv()
+
+    def send_piece(a, j):
+        if j:
+            arrived(a, j)
+        for kind, h, target in ((0, 0, rx), (3, 1, ry), (1, 1, rx), (2, 0, ry)):
+            c = hop2(a, j, kind, r, h, target, j == 0)
+            c.start()
+            started.append(c)
+
+    def forward_piece(a, j):
+        wait2(a, j, 0)
+        c = hop2(a, j, 4, rx, 0, ry, False)
+        c.start()
+        started.append(c)
+        wait2(a, j, 3)
+        c = hop2(a, j, 5, ry, 1, rx, False)
+        c.start()
+        started.append(c)
+
+    small = [(a, j) for j in range(Z) for a in (1, 2)]
+    for j in range(1, Z):
+        for a in (1, 2, 0):
+            first_hop(a, j)
+    for a in (1, 2):
+        send_piece(a, 0)
+    for a in (3, 4, 5):
+        first_hop(a, 1)
+    for a in range(6):
+        keep(source(a, z), place(a, z, r), a)
+    keep(resid_in, resid, 6)
+    keep(w_in, w, 7)
+    lag = 2
+    for i in range(2, len(small) + lag):
+        if i < len(small):
+            send_piece(*small[i])
+        if i == len(small) - 1:
+            for a in (3, 4, 5):
+                send_piece(a, 0)
+        forward_piece(*small[i - lag])
+    for j in range(2, Z - 1):
+        for a in (3, 4, 5):
+            first_hop(a, j)
+    for a, j in small:
+        for kind in (1, 2, 4, 5):
+            wait2(a, j, kind)
+    for j in range(1, Z):
+        arrived(0, j)
+    for c in locals_:
+        c.wait()
+
+    head_lam = lam[z]
+
+    def span(ref, n):
+        return ref[pl.ds(n * R, R)].reshape(R * T, VD)
+
+    @pl.loop(0, Z)
+    def _(i):
+        ho[i] = attention_block(
+            R,
+            T,
+            i,
+            r,
+            lambda b: q_sc[b],
+            lambda n: span(k_sc, n),
+            lambda n: span(v_sc, n),
+            head_lam,
+            head_gain[...],
+        )
+
+    copies = []
+    for j in range(1, Z):
+        c = remote(
+            ho.at[ahead[j]], heads.at[z], ho_sem.at[0, j], ho_sem.at[1, j], dev(ahead[j], r), t
+        )
+        c.start()
+        copies.append(c)
+    for a in (3, 4, 5):
+        first_hop(a, Z - 1)
+    heads[z] = ho[z]
+
+    big = [(a, j) for j in range(Z) for a in (3, 4, 5)]
+    big_lag = 3
+
+    def service(i):
+        if 3 <= i < len(big):
+            send_piece(*big[i])
+        if big_lag <= i < len(big) + big_lag:
+            forward_piece(*big[i - big_lag])
+
+    for i in range(3, 6):
+        service(i)
+
+    for c in copies:
+        c.wait()
+    NT = 512 if D % 512 == 0 else D
+    for h in range(2):
+        hh = (1 - t) if h == 0 else t
+        rows = pl.ds(pl.multiple_of(hh * H, 16), H)
+        left = jnp.concatenate([heads[n, rows, :] for n in range(Z)], axis=1)
+        for n in range(0, D, NT):
+            part[h, :, n : n + NT] = jnp.dot(
+                left, w[:, n : n + NT], preferred_element_type=jnp.float32
+            ).astype(jnp.bfloat16)
+        if h == 0:
+            swap = remote(part.at[0], got, swap_sem.at[0], swap_sem.at[1], me, 1 - t)
+            swap.start()
+    swap.wait()
+    own_rows = pl.ds(pl.multiple_of(t * H, 16), H)
+    first_val = resid[own_rows, :].astype(jnp.float32) + (
+        part[1].astype(jnp.float32) + got[...].astype(jnp.float32)
+    )
+    first[...] = first_val
+    norm_sc[...] = rms_rows(first_val, norm_gain[...])
+
+    def rows_of(zz, tt):
+        return all_sc.at[zz, tt]
+
+    copies = []
+    for j in range(1, Z):
+        c = remote(
+            norm_sc, rows_of(z, t), ag_sem.at[0, j], ag_sem.at[1, j], dev(ahead[j], r), t
+        )
+        c.start()
+        copies.append(c)
+    across = [remote(norm_sc, rows_of(z, t), core_sem.at[0, 0], core_sem.at[1, 0], me, 1 - t)]
+    across[0].start()
+    own = pltpu.make_async_copy(norm_sc, rows_of(z, t), local_sem.at[0])
+    own.start()
+
+    for i in range(6, len(big) + big_lag):
+        service(i)
+
+    for j in range(1, Z):
+        zz = behind[j]
+        remote(
+            norm_sc, rows_of(zz, t), ag_sem.at[0, j], ag_sem.at[1, j], dev(zz, r), t
+        ).wait_recv()
+        c = remote(rows_of(zz, t), rows_of(zz, t), core_sem.at[0, j], core_sem.at[1, j], me, 1 - t)
+        c.start()
+        across.append(c)
+    own.wait()
+    for a, j in big:
+        for kind in (1, 2, 4, 5):
+            wait2(a, j, kind)
+    for j in range(Z):
+        zz = behind[j]
+        remote(
+            rows_of(zz, t), rows_of(zz, 1 - t), core_sem.at[0, j], core_sem.at[1, j], me, 1 - t
+        ).wait_recv()
+
+    FT = 256 if width % 256 == 0 else LANE
+    DN = d_sc.shape[2]
+    low = first_block(z, share) * LANE
+    sent = []
+    order = [j % Z for j in range(1, Z + 1)]
+    for n, j in enumerate(order):
+        zz = ahead[j]
+        block = all_sc[zz].reshape(T, D)
+
+        @pl.loop(0, width // FT)
+        def _(f, block=block):
+            cols = pl.ds(pl.multiple_of(f * FT, FT), FT)
+            gate = jnp.dot(
+                block, g_sc[:, :, cols].reshape(D, FT), preferred_element_type=jnp.float32
+            )
+            up = jnp.dot(
+                block, u_sc[:, :, cols].reshape(D, FT), preferred_element_type=jnp.float32
+            )
+            unit = low + f * FT + lax.broadcasted_iota(jnp.int32, gate.shape, 1)
+            counted = (unit >= z * share) & (unit < (z + 1) * share)
+            value = jax.nn.silu(gate) * up
+            hidden[:, cols] = jnp.where(counted, value, 0.0).astype(jnp.bfloat16)
+
+        left = hidden[...]
+
+        @pl.loop(0, (Z * R) // 2)
+        def _(p, left=left, n=n):
+            right = jnp.concatenate([d_sc[2 * p], d_sc[2 * p + 1]], axis=1)
+            value = jnp.dot(left, right, preferred_element_type=jnp.float32).astype(jnp.bfloat16)
+            cols = pl.ds(pl.multiple_of(p * (2 * DN), 2 * DN), 2 * DN)
+            terms[n, :, :, cols] = value.reshape(2, H, 2 * DN)
+
+        c = remote(
+            terms.at[n, 1 - t], cross.at[n], cross_sem.at[0, n], cross_sem.at[1, n], me, 1 - t
+        )
+        c.start()
+        c.wait()
+        total = terms[n, t].astype(jnp.float32) + cross[n].astype(jnp.float32)
+        if j:
+            sums[j] = total.astype(jnp.bfloat16)
+            c = remote(
+                sums.at[j], landed.at[j], sum_sem.at[0, j], sum_sem.at[1, j], dev(zz, r), t
+            )
+            c.start()
+            sent.append(c)
+        else:
+            first[...] = first[...] + 0.5 * total
+    for c in sent:
+        c.wait()
+    total = landed[1].astype(jnp.float32)
+    for j in range(2, Z):
+        total = total + landed[j].astype(jnp.float32)
+    sums[0] = (first[...] + 0.5 * total).astype(jnp.bfloat16)
+    c = remote(sums.at[0], out.at[own_rows, :], out_sem.at[0], out_sem.at[1], me, 1 - t)
+    c.start()
+    own = pltpu.make_async_copy(sums.at[0], out.at[own_rows, :], local_sem.at[1])
+    own.start()
+    own.wait()
+    c.wait()
+    for c in started + copies + across:
+        c.wait_send()
+
+
+def columns_form(
+    resid,
+    queries,
+    keys,
+    values,
+    lambdas,
+    head_gain,
+    out_weight,
+    norm_gain,
+    gate_weight,
+    up_weight,
+    down_weight,
+):
+    Z = lambdas.shape[0]
+    S = lax.axis_size("sp")
+    R = S // Z
+    T, D = resid.shape
+    H = T // 2
+    W = gate_weight.shape[0]
+    DN = down_weight.shape[1]
+    share = gate_weight.shape[1] // Z
+    width = LANE * max(
+        -(-((zz + 1) * share) // LANE) - (zz * share) // LANE for zz in range(Z)
+    )
+    bf, f32 = jnp.bfloat16, jnp.float32
+    vm = pl.BlockSpec(memory_space=pltpu.VMEM)
+    hbm = pl.BlockSpec(memory_space=pl.ANY)
+    dma = pltpu.SemaphoreType.DMA
+
+    def kernel(*refs):
+        whole_kernel(Z, R, share, width, refs)
+
+    return pl.pallas_call(
+        kernel,
+        out_shape=jax.ShapeDtypeStruct((T, D), bf),
+        in_specs=[hbm] * 8 + [pl.BlockSpec(memory_space=pltpu.SMEM), vm, vm],
+        out_specs=vm,
+        scratch_shapes=[
+            pltpu.VMEM((Z, T, VD), bf),
+            pltpu.VMEM((S, T, VD), bf),
+            pltpu.VMEM((S, T, VD), bf),
+            pltpu.VMEM((S, W, width), bf),
+            pltpu.VMEM((S, W, width), bf),
+            pltpu.VMEM((S, width, DN), bf),
+            pltpu.VMEM((T, D), bf),
+            pltpu.VMEM(out_weight.shape, bf),
+            pltpu.VMEM((Z, T, VD), bf),
+            pltpu.VMEM((Z, T, VD), bf),
+            pltpu.VMEM((2, H, D), bf),
+            pltpu.VMEM((H, D), bf),
+            pltpu.VMEM((H, D), f32),
+            pltpu.VMEM((H, D), bf),
+            pltpu.VMEM((Z, 2, H, D), bf),
+            pltpu.VMEM((T, width), bf),
+            pltpu.VMEM((Z, 2, H, D), bf),
+            pltpu.VMEM((Z, H, D), bf),
+            pltpu.VMEM((Z, H, D), bf),
+            pltpu.VMEM((Z, H, D), bf),
+            dma((6, Z)),
+            dma((6, Z)),
+            dma((5, Z, 6)),
+            dma((5, Z, 6)),
+            dma((8,)),
+            dma((2, Z)),
+            dma((2,)),
+            dma((2, Z)),
+            dma((2, Z)),
+            dma((2, Z)),
+            dma((2, Z)),
+            dma((2,)),
+        ],
+        compiler_params=pltpu.CompilerParams(
+            collective_id=0, has_side_effects=True, vmem_limit_bytes=VMEM_LIMIT
+        ),
+    )(
+        queries,
+        keys,
+        values,
+        gate_weight,
+        up_weight,
+        down_weight,
+        resid,
+        out_weight,
+        lambdas,
+        head_gain.reshape(1, -1),
+        norm_gain.reshape(1, -1),
+    )
+
+
 def solution(mesh):
+    sp, tp = mesh.shape["sp"], mesh.shape["tp"]
+
+    def local(*args):
+        heads = args[4].shape[0]
+        tok_rows = args[1].shape[0]
+        columns = (
+            tp == 2
+            and heads > 2
+            and sp == 4 * heads
+            and args[10].shape[1] % LANE == 0
+            and args[8].shape[1] % (16 * heads) == 0
+            and tok_rows % 32 == 0
+        )
+        return (columns_form if columns else generic)(*args)
+
     return jax.shard_map(
         local,
         mesh=mesh,

time: 743 us -> 183 us (0.25)
  waiting for transfers between devices: 612 us -> 0 us
  Pallas kernels: 0 us -> 181 us
  matrix products: 55.5 us -> 0 us
  other arithmetic: 27.8 us -> 0 us
  local copies, waits for them, and re-layouts: 26 us -> 2.09 us
  between operations: 13.6 us -> 0.01 us
    all_gather x5 -> x0, waiting for transfers between devices: 593 us -> none  [the longest x1 183 us: local(): lax.all_gather(down_weight, 'sp', axis=1, tiled=True)]
    pallas_call x0 -> x1, Pallas kernels: none -> 181 us  [columns_form(): pl.pallas_call(kernel, out_shape=jax.ShapeDtypeStruct((T, D), bf), in_spe...]
    dot_general x11 -> x0, matrix products: 55.5 us -> none  [the longest x4 16.9 us: update(): jnp.einsum('qhcd,khcd->chqk', query_four, key_part, preferred_element_typ...]
    dynamic_slice x12 -> x0, local copies, waits for them, and re-layouts: 23.3 us -> none  [the longest x8 14.2 us: one_span(): lax.dynamic_slice_in_dim(value_rows, span_start, key_span, 0)]
    convert_element_type x6 -> x0, other arithmetic: 19.7 us -> none  [the longest x4 17.4 us: update(): expo.astype(jnp.bfloat16)]
    reduce_scatter x2 -> x0, waiting for transfers between devices: 16.9 us -> none  [the longest x1 9.04 us: local(): lax.psum_scatter(terms.astype(jnp.bfloat16), 'tp', scatter_dimension=0, t...]
  transfers between devices with their start and end apart: 7 -> 0, of which waited for: 7 -> 0; matrix products, arithmetic and copies ran while one was open for 1% -> 0% of each run, Pallas kernels for 0% -> 0%
where the time goes in v2:
time: 183 us
  Pallas kernels  181 us (99%)
  local copies, waits for them, and re-layouts  2.09 us (1%)
    pallas_call x1, Pallas kernels, columns_form(): pl.pallas_call(kernel, out_shape=jax.ShapeDtypeStruct((T, D), bf), in_spe...  181 us

profile of v2, /device:TPU:25, one launch (start us, length us, event | category | flops | bytes accessed | tf_op | source)
XLA Modules:
  0.0 182.9 jit_solution(2280375749935186649)
XLA Ops:
  0.0 180.8 %shard_map.109 = bf16[192,2048]{1,0:T(8,128)(2,1)} custom-call(bf16[192,512]{1,0:T(8,128)(2,1)} %refs_0_.1, bf16[192,512]{1,0:T(8,128)(2,1)} %refs_1_.1, bf16[192,512]{1,0:T(8,128)(2,1)} %refs_2_.1, bf16[128,2816]{1,0:T(8,128)(2,1)} %refs_3_.1, bf16[128,2816]{1,0:T(8,128)(2,1)} %refs_4_.1, bf16[2816,128]{1,0:T(8,128)(2,1)} %refs_5_.1, ...), custom_call_target="tpu_custom_call" | custom-call | tf_op jit(solution)/shard_map/pallas_call | solution.py:547
  180.8 2.1 %copy.13 = bf16[192,2048]{1,0:T(8,128)(2,1)} copy(bf16[192,2048]{1,0:T(8,128)(2,1)} %shard_map.109) | data formatting | bytes 1572864

commit v3 on v2

--- a/solution.py
+++ b/solution.py
@@ -326,21 +326,22 @@
         send_piece(a, 0)
     for a in (3, 4, 5):
         first_hop(a, 1)
+    for j in range(2, Z - 1):
+        for a in (3, 4):
+            first_hop(a, j)
     for a in range(6):
         keep(source(a, z), place(a, z, r), a)
     keep(resid_in, resid, 6)
     keep(w_in, w, 7)
     lag = 2
     for i in range(2, len(small) + lag):
+        if i in (2, 4, 6):
+            send_piece(2 + i // 2, 0)
         if i < len(small):
             send_piece(*small[i])
-        if i == len(small) - 1:
-            for a in (3, 4, 5):
-                send_piece(a, 0)
         forward_piece(*small[i - lag])
     for j in range(2, Z - 1):
-        for a in (3, 4, 5):
-            first_hop(a, j)
+        first_hop(5, j)
     for a, j in small:
         for kind in (1, 2, 4, 5):
             wait2(a, j, kind)
@@ -416,38 +417,91 @@
     def rows_of(zz, tt):
         return all_sc.at[zz, tt]
 
-    copies = []
-    for j in range(1, Z):
-        c = remote(
-            norm_sc, rows_of(z, t), ag_sem.at[0, j], ag_sem.at[1, j], dev(ahead[j], r), t
-        )
-        c.start()
-        copies.append(c)
-    across = [remote(norm_sc, rows_of(z, t), core_sem.at[0, 0], core_sem.at[1, 0], me, 1 - t)]
-    across[0].start()
+    def ag_hop(down, d):
+        zz = z + (d - 1) if down else z - (d - 1)
+        to = z - 1 if down else z + 1
+        return remote(
+            norm_sc if d == 1 else rows_of(zz, t),
+            rows_of(zz, t),
+            ag_sem.at[2 * down, d],
+            ag_sem.at[2 * down + 1, d],
+            dev(to, r),
+            t,
+        )
+
+    def sends(down, d):
+        return (z > 0) & (z + (d - 1) < Z) if down else (z + 1 < Z) & (z - (d - 1) >= 0)
+
+    def gets(down, d):
+        return z + d < Z if down else z - d >= 0
+
+    def origin(down, d):
+        return z + d if down else z - d
+
+    def to_core(down, d, tt):
+        rows = rows_of(origin(down, d), tt)
+        n = 2 * d + down
+        return remote(rows, rows, core_sem.at[0, n], core_sem.at[1, n], me, 1 - t)
+
+    def ag_start(d):
+        for down in (0, 1):
+
+            @pl.when(sends(down, d))
+            def _(down=down):
+                ag_hop(down, d).start()
+
+    def ag_step(d):
+        for down in (0, 1):
+
+            @pl.when(gets(down, d))
+            def _(down=down):
+                rows = rows_of(origin(down, d), t)
+                remote(
+                    rows, rows, ag_sem.at[2 * down, d], ag_sem.at[2 * down + 1, d], me, 1 - t
+                ).wait_recv()
+                if d < Z - 1:
+
+                    @pl.when(sends(down, d + 1))
+                    def _():
+                        ag_hop(down, d + 1).start()
+
+                to_core(down, d, t).start()
+
+    ag_start(1)
+    across = remote(norm_sc, rows_of(z, t), core_sem.at[0, 0], core_sem.at[1, 0], me, 1 - t)
+    across.start()
     own = pltpu.make_async_copy(norm_sc, rows_of(z, t), local_sem.at[0])
     own.start()
 
-    for i in range(6, len(big) + big_lag):
+    for i in range(6, len(big)):
         service(i)
-
-    for j in range(1, Z):
-        zz = behind[j]
-        remote(
-            norm_sc, rows_of(zz, t), ag_sem.at[0, j], ag_sem.at[1, j], dev(zz, r), t
-        ).wait_recv()
-        c = remote(rows_of(zz, t), rows_of(zz, t), core_sem.at[0, j], core_sem.at[1, j], me, 1 - t)
-        c.start()
-        across.append(c)
+    done = 1
+    for i in range(len(big), len(big) + big_lag):
+        if done < Z:
+            ag_step(done)
+            done += 1
+        service(i)
+    for d in range(done, Z):
+        ag_step(d)
     own.wait()
     for a, j in big:
         for kind in (1, 2, 4, 5):
             wait2(a, j, kind)
-    for j in range(Z):
-        zz = behind[j]
-        remote(
-            rows_of(zz, t), rows_of(zz, 1 - t), core_sem.at[0, j], core_sem.at[1, j], me, 1 - t
-        ).wait_recv()
+    across.wait_send()
+    remote(
+        norm_sc, rows_of(z, 1 - t), core_sem.at[0, 0], core_sem.at[1, 0], me, 1 - t
+    ).wait_recv()
+    for d in range(1, Z):
+        for down in (0, 1):
+
+            @pl.when(gets(down, d))
+            def _(down=down, d=d):
+                to_core(down, d, 1 - t).wait_recv()
+                to_core(down, d, t).wait_send()
+
+            @pl.when(sends(down, d))
+            def _(down=down, d=d):
+                ag_hop(down, d).wait_send()
 
     FT = 256 if width % 256 == 0 else LANE
     DN = d_sc.shape[2]
@@ -508,7 +562,7 @@
     own.start()
     own.wait()
     c.wait()
-    for c in started + copies + across:
+    for c in started:
         c.wait_send()
 
 
@@ -577,8 +631,8 @@
             dma((8,)),
             dma((2, Z)),
             dma((2,)),
-            dma((2, Z)),
-            dma((2, Z)),
+            dma((4, Z)),
+            dma((2, 2 * Z)),
             dma((2, Z)),
             dma((2, Z)),
             dma((2,)),

time: 183 us -> 173 us (0.945)
  Pallas kernels: 181 us -> 171 us
    pallas_call x1, Pallas kernels: 181 us -> 171 us  [columns_form(): pl.pallas_call(kernel, out_shape=jax.ShapeDtypeStruct((T, D), bf), in_spe...]
where the time goes in v3:
time: 173 us
  Pallas kernels  171 us (99%)
  local copies, waits for them, and re-layouts  2.09 us (1%)
    pallas_call x1, Pallas kernels, columns_form(): pl.pallas_call(kernel, out_shape=jax.ShapeDtypeStruct((T, D), bf), in_spe...  171 us

profile of v3, /device:TPU:25, one launch (start us, length us, event | category | flops | bytes accessed | tf_op | source)
XLA Modules:
  0.0 173.0 jit_solution(7091210822833750241)
XLA Ops:
  0.0 170.9 %shard_map.109 = bf16[192,2048]{1,0:T(8,128)(2,1)} custom-call(bf16[192,512]{1,0:T(8,128)(2,1)} %refs_0_.1, bf16[192,512]{1,0:T(8,128)(2,1)} %refs_1_.1, bf16[192,512]{1,0:T(8,128)(2,1)} %refs_2_.1, bf16[128,2816]{1,0:T(8,128)(2,1)} %refs_3_.1, bf16[128,2816]{1,0:T(8,128)(2,1)} %refs_4_.1, bf16[2816,128]{1,0:T(8,128)(2,1)} %refs_5_.1, ...), custom_call_target="tpu_custom_call" | custom-call | tf_op jit(solution)/shard_map/pallas_call | solution.py:601
  170.9 2.1 %copy.13 = bf16[192,2048]{1,0:T(8,128)(2,1)} copy(bf16[192,2048]{1,0:T(8,128)(2,1)} %shard_map.109) | data formatting | bytes 1572864

commit v4 on v3

--- a/solution.py
+++ b/solution.py
@@ -8,6 +8,7 @@
 QK = 64
 VD = 128
 LANE = 128
+LATE = 3
 VMEM_LIMIT = 60 * 1024 * 1024
 
 
@@ -342,6 +343,18 @@
         forward_piece(*small[i - lag])
     for j in range(2, Z - 1):
         first_hop(5, j)
+    big = [(a, j) for j in range(Z) for a in (3, 4, 5)]
+    big_lag = 3
+
+    def service(i):
+        if 3 <= i < len(big):
+            send_piece(*big[i])
+        if big_lag <= i < len(big) + big_lag:
+            forward_piece(*big[i - big_lag])
+
+    for i in range(3, 6):
+        service(i)
+
     for a, j in small:
         for kind in (1, 2, 4, 5):
             wait2(a, j, kind)
@@ -380,16 +393,7 @@
         first_hop(a, Z - 1)
     heads[z] = ho[z]
 
-    big = [(a, j) for j in range(Z) for a in (3, 4, 5)]
-    big_lag = 3
-
-    def service(i):
-        if 3 <= i < len(big):
-            send_piece(*big[i])
-        if big_lag <= i < len(big) + big_lag:
-            forward_piece(*big[i - big_lag])
-
-    for i in range(3, 6):
+    for i in range(6, 6 + LATE):
         service(i)
 
     for c in copies:
@@ -473,7 +477,7 @@
     own = pltpu.make_async_copy(norm_sc, rows_of(z, t), local_sem.at[0])
     own.start()
 
-    for i in range(6, len(big)):
+    for i in range(6 + LATE, len(big)):
         service(i)
     done = 1
     for i in range(len(big), len(big) + big_lag):

time: 173 us -> 159 us (0.919)
  Pallas kernels: 171 us -> 157 us
    pallas_call x1, Pallas kernels: 171 us -> 157 us  [columns_form(): pl.pallas_call(kernel, out_shape=jax.ShapeDtypeStruct((T, D), bf), in_spe...]
where the time goes in v4:
time: 159 us
  Pallas kernels  157 us (99%)
  local copies, waits for them, and re-layouts  2.09 us (1%)
    pallas_call x1, Pallas kernels, columns_form(): pl.pallas_call(kernel, out_shape=jax.ShapeDtypeStruct((T, D), bf), in_spe...  157 us

profile of v4, /device:TPU:25, one launch (start us, length us, event | category | flops | bytes accessed | tf_op | source)
XLA Modules:
  0.0 159.3 jit_solution(4159648375756751797)
XLA Ops:
  0.0 157.2 %shard_map.109 = bf16[192,2048]{1,0:T(8,128)(2,1)} custom-call(bf16[192,512]{1,0:T(8,128)(2,1)} %refs_0_.1, bf16[192,512]{1,0:T(8,128)(2,1)} %refs_1_.1, bf16[192,512]{1,0:T(8,128)(2,1)} %refs_2_.1, bf16[128,2816]{1,0:T(8,128)(2,1)} %refs_3_.1, bf16[128,2816]{1,0:T(8,128)(2,1)} %refs_4_.1, bf16[2816,128]{1,0:T(8,128)(2,1)} %refs_5_.1, ...), custom_call_target="tpu_custom_call" | custom-call | tf_op jit(solution)/shard_map/pallas_call | solution.py:605
  157.2 2.1 %copy.13 = bf16[192,2048]{1,0:T(8,128)(2,1)} copy(bf16[192,2048]{1,0:T(8,128)(2,1)} %shard_map.109) | data formatting | bytes 1572864
